TPU v7x, 32 devices: a whole 2x2x4 slice. The times are simulated.
32 devices in a mesh: sp: 4 (over z), tp: 4 (over y, x), dp: 2 (over core).
Axes of the slice: x: 2, y: 2, z: 4, core: 2. Of those that a mesh axis runs over, the one named last changes fastest.
Arguments:
- latent: bfloat16 [2, 3072, 2048], P('dp', ('sp', 'tp')), may hold values from -3 to 3
- cond: bfloat16 [2, 2048], P('dp', 'sp'), may hold values from -6 to 6
- cond_ctx: bfloat16 [2048], P('sp'), may hold values from -6 to 6
- context: bfloat16 [2, 512, 2048], P('dp', 'sp'), may hold values from -6 to 6
- norm_gain: bfloat16 [2048], replicated, may hold values from 0.099609375 to 1.8984375
- mod_shift: bfloat16 [2048, 2048], P('sp', 'tp'), may hold values from -0.125 to 0.125
- mod_scale: bfloat16 [2048, 2048], P('sp', 'tp'), may hold values from -0.125 to 0.125
- mod_gate: bfloat16 [2048, 2048], P('sp', 'tp'), may hold values from -0.125 to 0.125
- w_query: bfloat16 [2048, 1024], P(None, 'tp'), may hold values from -0.125 to 0.125
- w_key: bfloat16 [2048, 256], P(None, 'tp'), may hold values from -0.125 to 0.125
- w_value: bfloat16 [2048, 256], P(None, 'tp'), may hold values from -0.125 to 0.125
- q_gain: bfloat16 [64], replicated, may hold values from 1 to 5.5
- k_gain: bfloat16 [64], replicated, may hold values from 1 to 5.5
- ctx_lift: float32 [16], P('tp'), may hold values from 1 to 3
- w_out: bfloat16 [1024, 2048], replicated, may hold values from -1.5 to 1.5
Outputs:
- mixed: bfloat16 [2, 3072, 2048], P('dp', ('sp', 'tp'))
All inputs are finite; a program needn't handle non-finite values.
Results may differ from a plain program's by a relative error of at most 0.009.
The roundings to bfloat16 on the way count: a program that leaves them out, or rounds other values in their place, can miss the bound.
Values may be sent and summed in bfloat16 or wider, within the bound.
A program may use at most 64 MiB of HBM per device.

v0:
```python
import jax
import jax.numpy as jnp
from jax import lax
from jax.sharding import PartitionSpec as P

HD = 64
GRID_W = 128
EPS = 1e-06
THETA = 10000.0


def modulate(row_block, gain_vec, shift_rows, scale_rows):
    values = row_block.astype(jnp.float32)
    normed = (
        values
        * lax.rsqrt(jnp.mean(values * values, axis=-1, keepdims=True) + EPS)
        * gain_vec.astype(jnp.float32)
    )
    return (normed * (1.0 + scale_rows) + shift_rows).astype(jnp.bfloat16)


def head_norm(raw_proj, gain_vec):
    samples, tokens, width = raw_proj.shape
    pieces = raw_proj.reshape(samples, tokens, width // HD, HD)
    normed = (
        pieces
        * lax.rsqrt(jnp.mean(pieces * pieces, axis=-1, keepdims=True) + EPS)
        * gain_vec.astype(jnp.float32)
    )
    return normed.transpose(0, 2, 1, 3)


def rotate(vector, positions):
    pairs_count = vector.shape[-1] // 4
    grid_row = (positions // GRID_W).astype(jnp.float32)
    grid_col = (positions % GRID_W).astype(jnp.float32)
    inverse = THETA ** (-jnp.arange(pairs_count, dtype=jnp.float32) / pairs_count)
    angles = jnp.concatenate([grid_row[:, None] * inverse, grid_col[:, None] * inverse], axis=-1)
    cosine = jnp.cos(angles)
    sine_val = jnp.sin(angles)
    first_half = vector[..., 0::2]
    second_half = vector[..., 1::2]
    turned = jnp.stack(
        [
            first_half * cosine - second_half * sine_val,
            first_half * sine_val + second_half * cosine,
        ],
        axis=-1,
    )
    return turned.reshape(vector.shape)


def split_heads(rows):
    samples, tokens, width = rows.shape
    return rows.reshape(samples, tokens, width // HD, HD).transpose(0, 2, 1, 3)


def on_device(
    latent,
    cond,
    cond_ctx,
    context,
    norm_gain,
    mod_shift,
    mod_scale,
    mod_gate,
    w_query,
    w_key,
    w_value,
    q_gain,
    k_gain,
    ctx_lift,
    w_out,
):
    samples = latent.shape[0]
    active = jax.nn.silu(
        jnp.concatenate([cond, cond_ctx[None, :]], axis=0).astype(jnp.float32)
    ).astype(jnp.bfloat16)
    partial_mods = tuple(
        (
            jnp.dot(active, weight, preferred_element_type=jnp.float32)
            for weight in (mod_shift, mod_scale, mod_gate)
        )
    )
    summed = lax.psum(partial_mods, "sp")
    shift_rows, scale_rows, gate_rows = lax.all_gather(summed, "tp", axis=1, tiled=True)
    modulated = modulate(
        latent, norm_gain, shift_rows[:samples, None, :], scale_rows[:samples, None, :]
    )
    ctx_mod = modulate(context, norm_gain, shift_rows[samples], scale_rows[samples])
    q_width = w_query.shape[1]
    k_width = w_key.shape[1]
    w_joint = jnp.concatenate([w_query, w_key, w_value], axis=1)
    projected = jnp.einsum(
        "srd,dc->src",
        lax.all_gather(modulated, "tp", axis=1, tiled=True),
        w_joint,
        preferred_element_type=jnp.float32,
    )
    tokens = projected.shape[1]
    k_heads = k_width // HD
    group_size = q_width // k_width
    positions = lax.axis_index("sp") * tokens + jnp.arange(tokens, dtype=jnp.int32)
    queries = rotate(head_norm(projected[..., :q_width], q_gain), positions).astype(jnp.bfloat16)
    queries = queries.reshape(samples, k_heads, group_size, tokens, HD)
    key_rows = rotate(
        head_norm(projected[..., q_width : q_width + k_width], k_gain), positions
    ).astype(jnp.bfloat16)
    value_rows = split_heads(projected[..., q_width + k_width :].astype(jnp.bfloat16))
    ctx_proj = jnp.einsum(
        "srd,dc->src", ctx_mod, w_joint[:, q_width:], preferred_element_type=jnp.float32
    )
    ctx_keys = head_norm(ctx_proj[..., :k_width], k_gain).astype(jnp.bfloat16)
    ctx_values = split_heads(ctx_proj[..., k_width:].astype(jnp.bfloat16))
    lift_table = ctx_lift.reshape(1, k_heads, group_size, 1, 1)
    factor = HD ** (-0.5)

    def absorb(state_now, key_block, value_block, score_lift):
        best_old, weight_sum, accumulated = state_now
        scores = (
            jnp.einsum("skgtd,skrd->skgtr", queries, key_block, preferred_element_type=jnp.float32)
            * factor
            + score_lift
        )
        peak = jnp.maximum(best_old, jnp.max(scores, axis=-1))
        weights = jnp.exp(scores - peak[..., None])
        rescale = jnp.exp(best_old - peak)
        weight_sum = weight_sum * rescale + jnp.sum(weights, axis=-1)
        accumulated = accumulated * rescale[..., None] + jnp.einsum(
            "skgtr,skrd->skgtd",
            weights.astype(jnp.bfloat16),
            value_block,
            preferred_element_type=jnp.float32,
        )
        return (peak, weight_sum, accumulated)

    stat_shape = (samples, k_heads, group_size, tokens)
    state_now = (
        jnp.full(stat_shape, -1e30, jnp.float32),
        jnp.zeros(stat_shape, jnp.float32),
        jnp.zeros(stat_shape + (HD,), jnp.float32),
    )
    all_ctx_keys, all_ctx_values = (
        lax.all_gather(ctx_keys, "sp", axis=2, tiled=True),
        lax.all_gather(ctx_values, "sp", axis=2, tiled=True),
    )
    state_now = absorb(state_now, all_ctx_keys, all_ctx_values, lift_table)
    key_piece = lax.all_gather(key_rows, "sp", axis=2, tiled=True)
    value_piece = lax.all_gather(value_rows, "sp", axis=2, tiled=True)
    block_count = key_piece.shape[2] // tokens
    key_blocks = jnp.moveaxis(key_piece.reshape(samples, k_heads, block_count, tokens, HD), 2, 0)
    value_blocks = jnp.moveaxis(
        value_piece.reshape(samples, k_heads, block_count, tokens, HD), 2, 0
    )

    def step_block(carry, blocks):
        return (absorb(carry, blocks[0], blocks[1], 0.0), None)

    state_out, unused = lax.scan(step_block, state_now, (key_blocks, value_blocks))
    state_now = state_out
    best_old, weight_sum, accumulated = state_now
    attended = (accumulated / weight_sum[..., None]).astype(jnp.bfloat16)
    head_rows = attended.transpose(0, 3, 1, 2, 4).reshape(samples, tokens, q_width)
    projected_out = jnp.einsum(
        "srq,qd->srd",
        lax.all_to_all(head_rows, "tp", split_axis=1, concat_axis=2, tiled=True),
        w_out,
        preferred_element_type=jnp.float32,
    )
    return (latent.astype(jnp.float32) + gate_rows[:samples, None, :] * projected_out).astype(
        jnp.bfloat16
    )


def solution(mesh):
    placed = (
        P("dp", ("sp", "tp"), None),
        P("dp", "sp"),
        P("sp"),
        P("dp", "sp", None),
        P(),
        P("sp", "tp"),
        P("sp", "tp"),
        P("sp", "tp"),
        P(None, "tp"),
        P(None, "tp"),
        P(None, "tp"),
        P(),
        P(),
        P("tp"),
        P(),
    )
    return jax.shard_map(
        on_device,
        mesh=mesh,
        in_specs=placed,
        out_specs=P("dp", ("sp", "tp"), None),
        check_vma=False,
    )
```

profile of v0, /device:TPU:0, one launch (start us, length us, event | category | flops | bytes accessed | tf_op | source)
XLA Modules:
  0.0 190.3 jit_solution(14167755606228791362)
XLA Ops:
  8.4 1.2 fusion.96
  10.9 20.5 %all-reduce = (f32[2,512]{1,0:T(2,128)S(1)}, f32[2,512]{1,0:T(2,128)S(1)}, f32[2,512]{1,0:T(2,128)S(1)}) all-reduce(f32[2,512]{1,0:T(2,128)S(1)} %fusion.94, f32[2,512]{1,0:T(2,128)S(1)} %fusion.96, f32[2,512]{1,0:T(2,128)S(1)} %fusion.98), channel_id=1, replica_groups=mesh['sp'=4,'tp'=4,'dp'=2] {'sp'}, use_global_device_ids=true, to_apply=%region_3.4 | all-reduce | flops 3072 | bytes 24576 | tf_op jit(solution)/shard_map/psum | solution.py:85
  31.4 8.2 %all_gather.25 = f32[2,2048]{1,0:T(2,128)S(1)} all-gather(f32[2,512]{1,0:T(2,128)S(1)} %get-tuple-element.88), channel_id=1, replica_groups=mesh['sp'=4,'tp'=4,'dp'=2] {'tp'}, dimensions={1}, use_global_device_ids=true | all-gather | bytes 20480 | tf_op jit(solution)/shard_map/all_gather | solution.py:86
  39.6 8.2 %all_gather.26 = f32[2,2048]{1,0:T(2,128)S(1)} all-gather(f32[2,512]{1,0:T(2,128)S(1)} %get-tuple-element.87), channel_id=1, replica_groups=mesh['sp'=4,'tp'=4,'dp'=2] {'tp'}, dimensions={1}, use_global_device_ids=true | all-gather | bytes 20480 | tf_op jit(solution)/shard_map/all_gather | solution.py:86
  48.4 1.4 fusion.31
  49.8 2.4 %fusion.35 = bf16[1,192,2048]{2,1,0:T(8,128)(2,1)} fusion(bf16[1,192,2048]{2,1,0:T(8,128)(2,1)} %param.17, f32[2048]{0:T(1024)S(1)} %bitcast.173, f32[2048]{0:T(1024)S(1)} %bitcast.172, f32[2048]{0:T(1024)S(1)} %convert_element_type.119, f32[192]{0:T(256)S(1)} %add_rsqrt_fusion.2), kind=kLoop, calls=%fused_computation.39 | loop fusion | flops 2359296 | bytes 1598208 | tf_op jit(solution)/shard_map/convert_element_type | solution.py:19
  53.6 12.0 %all_gather.28 = bf16[1,1,512,64]{2,3,1,0:T(8,128)(2,1)S(1)} all-gather(bf16[1,1,128,64]{2,3,1,0:T(8,128)(2,1)S(1)} %fusion.77), channel_id=1, replica_groups=mesh['sp'=4,'tp'=4,'dp'=2] {'sp'}, dimensions={2}, use_global_device_ids=true | all-gather | bytes 81920 | tf_op jit(solution)/shard_map/all_gather | solution.py:144
  65.7 12.6 %all-gather = bf16[1,512,64]{1,2,0:T(8,128)(2,1)} all-gather(bf16[1,128,64]{1,2,0:T(8,128)(2,1)S(1)} %slice.80), channel_id=2, replica_groups=mesh['sp'=4,'tp'=4,'dp'=2] {'sp'}, dimensions={1}, use_global_device_ids=true | all-gather | bytes 81920 | tf_op jit(solution)/shard_map/all_gather | solution.py:145
  80.1 13.4 %all-gather.4.cloned.1.call-done = bf16[1,768,2048]{2,1,0:T(8,128)(2,1)} async-done(((bf16[1,192,2048]{2,1,0:T(8,128)(2,1)}), bf16[1,768,2048]{2,1,0:T(8,128)(2,1)}) %all-gather.4.cloned.1.call-update) | async-done | bytes 3145744 | tf_op jit(solution)/shard_map/all_gather | solution.py:96
  93.5 3.7 %fusion.41 = f32[1,768,384]{1,2,0:T(8,128)S(1)} fusion(bf16[2048,64]{1,0:T(8,128)(2,1)S(1)} %copy.47, bf16[2048,64]{1,0:T(8,128)(2,1)S(1)} %copy.46, bf16[2048,256]{1,0:T(8,128)(2,1)} %param.25, bf16[1,768,2048]{2,1,0:T(8,128)(2,1)} %all-gather.4.cloned.1.call-done), kind=kOutput, calls=%fused_computation.45 | convolution fusion | flops 1212678144 | bytes 5898240 | tf_op jit(solution)/shard_map/srd,dc->src/dot_general | solution.py:94
  101.3 14.6 %all_gather.30 = bf16[1,1,3072,64]{2,3,1,0:T(8,128)(2,1)S(1)} all-gather(bf16[1,1,768,64]{2,3,1,0:T(8,128)(2,1)S(1)} %convert_element_type.131), channel_id=1, replica_groups=mesh['sp'=4,'tp'=4,'dp'=2] {'sp'}, dimensions={2}, use_global_device_ids=true | all-gather | bytes 491520 | tf_op jit(solution)/shard_map/all_gather | solution.py:148
  117.0 2.6 %copy-done.1 = f32[4,768,512]{1,2,0:T(8,128)} copy-done((f32[4,768,512]{1,2,0:T(8,128)}, f32[4,768,512]{1,2,0:T(8,128)S(1)}, u32[]{:S(2)}) %copy-start.1) | copy-done | bytes 6291480
  119.6 1.3 fusion.23
  120.9 15.5 %all-gather.1 = bf16[1,3072,64]{1,2,0:T(8,128)(2,1)S(1)} all-gather(bf16[1,768,64]{1,2,0:T(8,128)(2,1)S(1)} %slice.79), channel_id=3, replica_groups=mesh['sp'=4,'tp'=4,'dp'=2] {'sp'}, dimensions={1}, use_global_device_ids=true | all-gather | bytes 491520 | tf_op jit(solution)/shard_map/all_gather | solution.py:149
  136.8 4.3 %fusion.49 = f32[1,1,4,768,64]{3,4,2,1,0:T(8,128)S(1)} fusion(f32[4,768,512]{1,2,0:T(8,128)} %copy-done.1, f32[4,768]{1,0:T(4,128)S(1)} %get-tuple-element.106, f32[4]{0:T(128)S(1)} %copy-done.7, f32[4,768]{1,0:T(4,128)S(1)} %get-tuple-element.104, bf16[1,512,64]{1,2,0:T(8,128)(2,1)S(1)} %copy-done.6), kind=kOutput, calls=%fused_computation.49 | convolution fusion | flops 207814656 | bytes 7168016 | tf_op jit(solution)/shard_map/skgtr,skrd->skgtd/dot_general | solution.py:129
  141.0 19.7 %while.14 = (s32[]{:T(128)}, f32[1,1,4,768]{3,2,1,0:T(4,128)S(1)}, f32[1,1,4,768]{3,2,1,0:T(4,128)S(1)}, f32[1,1,4,768,64]{3,4,2,1,0:T(8,128)S(1)}, bf16[4,1,1,7...) while((s32[]{:T(128)}, f32[1,1,4,768]{3,2,1,0:T(4,128)S(1)}, ...), condition=%wide.region_13.14_spmd, body=%wide.region_10.13_spmd.sunk | while | flops 623256576 | bytes 30670940 | solution.py:159
  141.1 1.4 bitcast_reduce_fusion.2
  142.5 1.9 fusion.116
  144.4 1.6 fusion.115
  146.0 1.4 bitcast_reduce_fusion.2
  147.4 1.9 fusion.116
  149.3 1.6 fusion.115
  150.9 1.4 bitcast_reduce_fusion.2
  152.4 1.9 fusion.116
  154.3 1.6 fusion.115
  155.9 1.4 bitcast_reduce_fusion.2
  157.3 1.9 fusion.116
  159.2 1.6 fusion.115
  162.0 3.0 %reduce.15 = bf16[768,256]{1,0:T(8,128)(2,1)S(1)} reduce(bf16[768,1,256]{2,1,0:T(2,128)(2,1)S(1)} %bitcast.162, bf16[]{:T(256)} %broadcast.433), dimensions={1}, to_apply=%bitcast.124.reduce_sub_computation | reduce | bytes 786434
  165.9 3.5 %all-to-all-start = ((bf16[4,2,24576]{2,1,0:T(2,128)(2,1)}), bf16[4,2,24576]{2,1,0:T(2,128)(2,1)S(1)}, u32[]{:S(2)}, u32[]{:S(2)}) async-start(bf16[4,2,24576]{2,1,0:T(2,128)(2,1)} %reshape.683), calls=%async_computation | async-start | bytes 786432 | tf_op jit(solution)/shard_map/all_to_all | solution.py:166
  169.4 9.1 %all_gather.24 = f32[2,2048]{1,0:T(2,128)S(1)} all-gather(f32[2,512]{1,0:T(2,128)S(1)} %get-tuple-element.89), channel_id=1, replica_groups=mesh['sp'=4,'tp'=4,'dp'=2] {'tp'}, dimensions={1}, use_global_device_ids=true | all-gather | bytes 20480 | tf_op jit(solution)/shard_map/all_gather | solution.py:86
  179.3 4.1 %fusion.30 = bf16[1,192,2048]{2,1,0:T(8,128)(2,1)} fusion(bf16[192,1024]{1,0:T(8,128)(2,1)S(1)} %bitcast.171, bf16[1024,2048]{1,0:T(8,128)(2,1)} %param.31, bf16[1,192,2048]{2,1,0:T(8,128)(2,1)S(1)} %copy-done.2, f32[2048]{0:T(1024)S(1)} %bitcast.174), kind=kOutput, calls=%fused_computation.32 | convolution fusion | flops 806879232 | bytes 6168576 | tf_op jit(solution)/shard_map/srq,qd->srd/dot_general | solution.py:164
  (92 shorter events, 15.4 us)
Async XLA Ops:
  6.5 1.0 copy-start
  6.5 45.7 %copy-start.5 = (bf16[2048,64]{0,1:T(8,128)(2,1)S(1)}, bf16[2048,64]{0,1:T(8,128)(2,1)}, u32[]{:S(2)}) copy-start(bf16[2048,64]{0,1:T(8,128)(2,1)} %param.26) | copy-start | bytes 786436
  6.5 46.0 %copy-start.4 = (bf16[2048,64]{0,1:T(8,128)(2,1)S(1)}, bf16[2048,64]{0,1:T(8,128)(2,1)}, u32[]{:S(2)}) copy-start(bf16[2048,64]{0,1:T(8,128)(2,1)} %param.27) | copy-start | bytes 786436
  6.5 46.3 %copy-start.8 = (bf16[64]{0:T(256)(128)(2,1)S(1)}, bf16[64]{0:T(256)(128)(2,1)}, u32[]{:S(2)}) copy-start(bf16[64]{0:T(256)(128)(2,1)} %param.29) | copy-start | bytes 388
  6.5 46.3 %copy-start.9 = (bf16[64]{0:T(256)(128)(2,1)S(1)}, bf16[64]{0:T(256)(128)(2,1)}, u32[]{:S(2)}) copy-start(bf16[64]{0:T(256)(128)(2,1)} %param.28) | copy-start | bytes 388
  6.5 46.3 %copy-start.3 = (bf16[1,128,2048]{2,1,0:T(8,128)(2,1)S(1)}, bf16[1,128,2048]{2,1,0:T(8,128)(2,1)}, u32[]{:S(2)}) copy-start(bf16[1,128,2048]{2,1,0:T(8,128)(2,1)} %param.20) | copy-start | bytes 1572868
  6.6 86.9 %all-gather.4.cloned.1.call-start = ((), (), s32[]{:S(2)}) async-start(), calls=%async_computation.1 | async-start | bytes 3932160 | tf_op jit(solution)/shard_map/all_gather | solution.py:96
  97.5 18.4 %copy-start.7 = (f32[4]{0:T(128)S(1)}, f32[4]{0:T(128)}, u32[]{:S(2)}) copy-start(f32[4]{0:T(128)} %param.30) | copy-start | bytes 52
  116.9 2.7 %copy-start.1 = (f32[4,768,512]{1,2,0:T(8,128)}, f32[4,768,512]{1,2,0:T(8,128)S(1)}, u32[]{:S(2)}) copy-start(f32[4,768,512]{1,2,0:T(8,128)S(1)} %get-tuple-element.114) | copy-start | bytes 18874372
  117.0 19.8 %copy-start.6 = (bf16[1,512,64]{1,2,0:T(8,128)(2,1)S(1)}, bf16[1,512,64]{1,2,0:T(8,128)(2,1)}, u32[]{:S(2)}) copy-start(bf16[1,512,64]{1,2,0:T(8,128)(2,1)} %all-gather) | copy-start | bytes 196612
  160.8 18.5 %copy-start.2 = (bf16[1,192,2048]{2,1,0:T(8,128)(2,1)S(1)}, bf16[1,192,2048]{2,1,0:T(8,128)(2,1)}, u32[]{:S(2)}) copy-start(bf16[1,192,2048]{2,1,0:T(8,128)(2,1)} %param.17) | copy-start | bytes 2359300
  165.9 12.5 %all-to-all-start = ((bf16[4,2,24576]{2,1,0:T(2,128)(2,1)}), bf16[4,2,24576]{2,1,0:T(2,128)(2,1)S(1)}, u32[]{:S(2)}, u32[]{:S(2)}) async-start(bf16[4,2,24576]{2,1,0:T(2,128)(2,1)} %reshape.683), calls=%async_computation | async-start | bytes 786432 | tf_op jit(solution)/shard_map/all_to_all | solution.py:166
Sparse Core Ops, SparseCore 0:
  52.3 41.0 all-gather.3
where the time goes:
time: 191 us; the launch traced here: 190 us
  blocking collectives  101 us (53%)
  matrix products  30 us (16%)
  other arithmetic  20 us (10%)
  between operations  13.8 us (7%)
  waiting for transfers between devices  13.4 us (7%)
  local copies, waits for them, and re-layouts  8.75 us (5%)
  starting transfers between devices  3.5 us (2%)
    all_gather x3, blocking collectives, on_device(): lax.all_gather(summed, 'tp', axis=1, tiled=True)  25.4 us
    psum x1, blocking collectives, on_device(): summed = lax.psum(partial_mods, 'sp')  20.5 us
    all_gather x1, blocking collectives, on_device(): value_piece = lax.all_gather(value_rows, 'sp', axis=2, tiled=True)  15.5 us
    all_gather x1, blocking collectives, on_device(): key_piece = lax.all_gather(key_rows, 'sp', axis=2, tiled=True)  14.6 us
    all_gather x1, waiting for transfers between devices, on_device(): lax.all_gather(modulated, 'tp', axis=1, tiled=True)  13.4 us
    all_gather x1, blocking collectives, on_device(): lax.all_gather(ctx_values, 'sp', axis=2, tiled=True)  12.6 us
    all_gather x1, blocking collectives, on_device(): lax.all_gather(ctx_keys, 'sp', axis=2, tiled=True)  12 us
    dot_general x5, matrix products, absorb(): jnp.einsum('skgtr,skrd->skgtd', weights.astype(jnp.bfloat16), value_block...  11.7 us
  transfers between devices with their start and end apart: 2, of which 1 were waited for; matrix products, arithmetic and copies ran while one was open for 2% of the time, Pallas kernels for 0%

commit v1 on v0

--- a/solution.py
+++ b/solution.py
@@ -146,7 +146,12 @@
     )
     state_now = absorb(state_now, all_ctx_keys, all_ctx_values, lift_table)
     key_piece = lax.all_gather(key_rows, "sp", axis=2, tiled=True)
-    value_piece = lax.all_gather(value_rows, "sp", axis=2, tiled=True)
+    ring = [value_rows]
+    for hop in range(3):
+        ring.append(lax.ppermute(ring[-1], "sp", [(dev, (dev + 1) % 4) for dev in range(4)]))
+    value_piece = jnp.roll(
+        jnp.concatenate(ring[::-1], axis=2), (lax.axis_index("sp") + 1) * ring[0].shape[2], axis=2
+    )
     block_count = key_piece.shape[2] // tokens
     key_blocks = jnp.moveaxis(key_piece.reshape(samples, k_heads, block_count, tokens, HD), 2, 0)
     value_blocks = jnp.moveaxis(

time: 191 us -> 180 us (0.942)
  blocking collectives: 101 us -> 86.2 us
  starting transfers between devices: 3.5 us -> 6.58 us
  waiting for transfers between devices: 13.4 us -> 16.2 us
    all_gather x1 -> x0, blocking collectives: 15.5 us -> none  [on_device(): value_piece = lax.all_gather(value_rows, 'sp', axis=2, tiled=True)]
    ppermute x0 -> x3, waiting for transfers between devices: none -> 3.94 us  [on_device(): lax.ppermute(ring[-1], 'sp', [(dev, (dev + 1) % 4) for dev in range(4)])]
    ppermute x0 -> x3, starting transfers between devices: none -> 3.08 us  [on_device(): lax.ppermute(ring[-1], 'sp', [(dev, (dev + 1) % 4) for dev in range(4)])]
    dot_general x5, matrix products: 11.7 us -> 8.94 us  [absorb(): jnp.einsum('skgtr,skrd->skgtd', weights.astype(jnp.bfloat16), value_block...]
    unnamed x27 -> x38, local copies, waits for them, and re-layouts: 5.28 us -> 2.74 us
  transfers between devices with their start and end apart: 2 -> 5, of which waited for: 1 -> 2; matrix products, arithmetic and copies ran while one was open for 2% -> 7% of each run, Pallas kernels for 0% -> 0%
where the time goes in v1:
time: 180 us
  blocking collectives  86.2 us (48%)
  matrix products  28.1 us (16%)
  other arithmetic  21.1 us (12%)
  waiting for transfers between devices  16.2 us (9%)
  between operations  13.9 us (8%)
  local copies, waits for them, and re-layouts  7.38 us (4%)
  starting transfers between devices  6.58 us (4%)
    all_gather x3, blocking collectives, on_device(): lax.all_gather(summed, 'tp', axis=1, tiled=True)  25.4 us
    psum x1, blocking collectives, on_device(): summed = lax.psum(partial_mods, 'sp')  20.5 us
    all_gather x1, blocking collectives, on_device(): key_piece = lax.all_gather(key_rows, 'sp', axis=2, tiled=True)  15.1 us
    all_gather x1, blocking collectives, on_device(): lax.all_gather(ctx_keys, 'sp', axis=2, tiled=True)  12.6 us
    all_gather x1, blocking collectives, on_device(): lax.all_gather(ctx_values, 'sp', axis=2, tiled=True)  12.6 us
    all_gather x1, waiting for transfers between devices, on_device(): lax.all_gather(modulated, 'tp', axis=1, tiled=True)  12.3 us
    dot_general x5, matrix products, absorb(): jnp.einsum('skgtr,skrd->skgtd', weights.astype(jnp.bfloat16), value_block...  8.94 us
    dot_general x5, matrix products, absorb(): jnp.einsum('skgtd,skrd->skgtr', queries, key_block, preferred_element_typ...  7.6 us
  transfers between devices with their start and end apart: 5, of which 2 were waited for; matrix products, arithmetic and copies ran while one was open for 7% of the time, Pallas kernels for 0%

profile of v1, /device:TPU:0, one launch (start us, length us, event | category | flops | bytes accessed | tf_op | source)
XLA Modules:
  0.0 179.6 jit_solution(9768121297032490954)
XLA Ops:
  10.9 20.5 %all-reduce = (f32[2,512]{1,0:T(2,128)S(1)}, f32[2,512]{1,0:T(2,128)S(1)}, f32[2,512]{1,0:T(2,128)S(1)}) all-reduce(f32[2,512]{1,0:T(2,128)S(1)} %fusion.95, f32[2,512]{1,0:T(2,128)S(1)} %fusion.97, f32[2,512]{1,0:T(2,128)S(1)} %fusion.99), channel_id=1, replica_groups=mesh['sp'=4,'tp'=4,'dp'=2] {'sp'}, use_global_device_ids=true, to_apply=%region_3.4 | all-reduce | flops 3072 | bytes 24576 | tf_op jit(solution)/shard_map/psum | solution.py:85
  31.4 8.2 %all_gather.22 = f32[2,2048]{1,0:T(2,128)S(1)} all-gather(f32[2,512]{1,0:T(2,128)S(1)} %get-tuple-element.81), channel_id=1, replica_groups=mesh['sp'=4,'tp'=4,'dp'=2] {'tp'}, dimensions={1}, use_global_device_ids=true | all-gather | bytes 20480 | tf_op jit(solution)/shard_map/all_gather | solution.py:86
  39.6 8.2 %all_gather.23 = f32[2,2048]{1,0:T(2,128)S(1)} all-gather(f32[2,512]{1,0:T(2,128)S(1)} %get-tuple-element.80), channel_id=1, replica_groups=mesh['sp'=4,'tp'=4,'dp'=2] {'tp'}, dimensions={1}, use_global_device_ids=true | all-gather | bytes 20480 | tf_op jit(solution)/shard_map/all_gather | solution.py:86
  48.4 1.4 fusion.31
  49.8 2.4 %fusion.35 = bf16[1,192,2048]{2,1,0:T(8,128)(2,1)} fusion(bf16[1,192,2048]{2,1,0:T(8,128)(2,1)} %param.17, f32[2048]{0:T(1024)S(1)} %bitcast.183, f32[2048]{0:T(1024)S(1)} %bitcast.182, f32[2048]{0:T(1024)S(1)} %convert_element_type.119, f32[192]{0:T(256)S(1)} %add_rsqrt_fusion.2), kind=kLoop, calls=%fused_computation.39 | loop fusion | flops 2359296 | bytes 1598208 | tf_op jit(solution)/shard_map/convert_element_type | solution.py:19
  54.1 12.6 %all_gather.25 = bf16[1,1,512,64]{2,3,1,0:T(8,128)(2,1)} all-gather(bf16[1,1,128,64]{2,3,1,0:T(8,128)(2,1)S(1)} %fusion.78), channel_id=1, replica_groups=mesh['sp'=4,'tp'=4,'dp'=2] {'sp'}, dimensions={2}, use_global_device_ids=true | all-gather | bytes 81920 | tf_op jit(solution)/shard_map/all_gather | solution.py:144
  66.8 12.6 %all-gather = bf16[1,512,64]{1,2,0:T(8,128)(2,1)} all-gather(bf16[1,128,64]{1,2,0:T(8,128)(2,1)S(1)} %slice.81), channel_id=2, replica_groups=mesh['sp'=4,'tp'=4,'dp'=2] {'sp'}, dimensions={1}, use_global_device_ids=true | all-gather | bytes 81920 | tf_op jit(solution)/shard_map/all_gather | solution.py:145
  81.2 12.3 %all-gather.3.cloned.1.call-done = bf16[1,768,2048]{2,1,0:T(8,128)(2,1)} async-done(((bf16[1,192,2048]{2,1,0:T(8,128)(2,1)}), bf16[1,768,2048]{2,1,0:T(8,128)(2,1)}) %all-gather.3.cloned.1.call-update) | async-done | bytes 3145744 | tf_op jit(solution)/shard_map/all_gather | solution.py:96
  93.5 3.7 %fusion.41 = f32[1,768,384]{1,2,0:T(8,128)S(1)} fusion(bf16[2048,64]{1,0:T(8,128)(2,1)S(1)} %copy.46, bf16[2048,64]{1,0:T(8,128)(2,1)S(1)} %copy.45, bf16[2048,256]{1,0:T(8,128)(2,1)} %param.25, bf16[1,768,2048]{2,1,0:T(8,128)(2,1)} %all-gather.3.cloned.1.call-done), kind=kOutput, calls=%fused_computation.45 | convolution fusion | flops 1212678144 | bytes 5898240 | tf_op jit(solution)/shard_map/srd,dc->src/dot_general | solution.py:94
  99.3 1.5 collective-permute-start
  102.5 1.9 %fusion.21 = (f32[4,768]{1,0:T(4,128)S(1)}, f32[4,768,512]{1,2,0:T(8,128)S(1)}) fusion(f32[4]{0:T(128)S(1)} %copy-done.8, bf16[4,768,64]{1,2,0:T(8,128)(2,1)S(1)} %convert_element_type.125, bf16[1,1,512,64]{2,3,1,0:T(8,128)(2,1)} %all_gather.25), kind=kOutput, calls=%fused_computation.23 | convolution fusion | flops 206042112 | bytes 6762512 | tf_op jit(solution)/shard_map/skgtd,skrd->skgtr/dot_general | solution.py:121
  105.8 1.5 fusion.49
  108.5 1.5 collective-permute-start.1
  111.0 3.9 %collective-permute-done.1 = bf16[1,1,768,64]{2,3,1,0:T(8,128)(2,1)S(1)} collective-permute-done((bf16[1,1,768,64]{2,3,1,0:T(8,128)(2,1)S(1)}, bf16[1,1,768,64]{2,3,1,0:T(8,128)(2,1)S(1)}, u32[]{:S(2)}, u32[]{:S(2)}) %collective-permute-start.1) | collective-permute-done | bytes 98336 | tf_op jit(solution)/shard_map/ppermute | solution.py:151
  114.9 15.1 %all_gather.27 = bf16[1,1,3072,64]{2,3,1,0:T(8,128)(2,1)S(1)} all-gather(bf16[1,1,768,64]{2,3,1,0:T(8,128)(2,1)S(1)} %convert_element_type.131), channel_id=1, replica_groups=mesh['sp'=4,'tp'=4,'dp'=2] {'sp'}, dimensions={2}, use_global_device_ids=true | all-gather | bytes 491520 | tf_op jit(solution)/shard_map/all_gather | solution.py:148
  130.4 19.7 %while.14 = (s32[]{:T(128)}, f32[1,1,4,768]{3,2,1,0:T(4,128)S(1)}, f32[1,1,4,768]{3,2,1,0:T(4,128)S(1)}, f32[1,1,4,768,64]{3,4,2,1,0:T(8,128)S(1)}, bf16[4,1,1,7...) while((s32[]{:T(128)}, f32[1,1,4,768]{3,2,1,0:T(4,128)S(1)}, ...), condition=%wide.region_13.14_spmd, body=%wide.region_10.13_spmd.sunk | while | flops 623256576 | bytes 30670940 | solution.py:164
  130.4 1.4 bitcast_reduce_fusion.2
  131.9 1.9 %fusion.117 = f32[1,1,4,768,64]{3,4,2,1,0:T(8,128)S(1)} fusion(f32[768,4,768]{2,0,1:T(8,128)S(1)} %get-tuple-element.159, f32[4,768]{1,0:T(4,128)S(1)} %bitcast.168, f32[1,1,4,768,64]{3,4,2,1,0:T(8,128)S(1)} %get-tuple-element.172, f32[4,768]{1,0:T(4,128)S(1)} %get-tuple-element.160, bf16[4,1,1,768,64]{3,4,2,1,0:T(8,128)(2,1)S(1)} %get-tuple-element.183, ...), kind=kOutput, calls=%fused_computation.7.clone.1 | convolution fusion | flops 309460992 | bytes 11132932 | tf_op jit(solution)/shard_map/while/body/eval_jaxpr/skgtr,skrd->skgtd/dot_general | solution.py:129
  133.8 1.6 fusion.116
  135.4 1.4 bitcast_reduce_fusion.2
  136.8 1.9 %fusion.117 = f32[1,1,4,768,64]{3,4,2,1,0:T(8,128)S(1)} fusion(f32[768,4,768]{2,0,1:T(8,128)S(1)} %get-tuple-element.159, f32[4,768]{1,0:T(4,128)S(1)} %bitcast.168, f32[1,1,4,768,64]{3,4,2,1,0:T(8,128)S(1)} %get-tuple-element.172, f32[4,768]{1,0:T(4,128)S(1)} %get-tuple-element.160, bf16[4,1,1,768,64]{3,4,2,1,0:T(8,128)(2,1)S(1)} %get-tuple-element.183, ...), kind=kOutput, calls=%fused_computation.7.clone.1 | convolution fusion | flops 309460992 | bytes 11132932 | tf_op jit(solution)/shard_map/while/body/eval_jaxpr/skgtr,skrd->skgtd/dot_general | solution.py:129
  138.7 1.6 fusion.116
  140.3 1.4 bitcast_reduce_fusion.2
  141.8 1.9 %fusion.117 = f32[1,1,4,768,64]{3,4,2,1,0:T(8,128)S(1)} fusion(f32[768,4,768]{2,0,1:T(8,128)S(1)} %get-tuple-element.159, f32[4,768]{1,0:T(4,128)S(1)} %bitcast.168, f32[1,1,4,768,64]{3,4,2,1,0:T(8,128)S(1)} %get-tuple-element.172, f32[4,768]{1,0:T(4,128)S(1)} %get-tuple-element.160, bf16[4,1,1,768,64]{3,4,2,1,0:T(8,128)(2,1)S(1)} %get-tuple-element.183, ...), kind=kOutput, calls=%fused_computation.7.clone.1 | convolution fusion | flops 309460992 | bytes 11132932 | tf_op jit(solution)/shard_map/while/body/eval_jaxpr/skgtr,skrd->skgtd/dot_general | solution.py:129
  143.6 1.6 fusion.116
  145.2 1.4 bitcast_reduce_fusion.2
  146.7 1.9 %fusion.117 = f32[1,1,4,768,64]{3,4,2,1,0:T(8,128)S(1)} fusion(f32[768,4,768]{2,0,1:T(8,128)S(1)} %get-tuple-element.159, f32[4,768]{1,0:T(4,128)S(1)} %bitcast.168, f32[1,1,4,768,64]{3,4,2,1,0:T(8,128)S(1)} %get-tuple-element.172, f32[4,768]{1,0:T(4,128)S(1)} %get-tuple-element.160, bf16[4,1,1,768,64]{3,4,2,1,0:T(8,128)(2,1)S(1)} %get-tuple-element.183, ...), kind=kOutput, calls=%fused_computation.7.clone.1 | convolution fusion | flops 309460992 | bytes 11132932 | tf_op jit(solution)/shard_map/while/body/eval_jaxpr/skgtr,skrd->skgtd/dot_general | solution.py:129
  148.6 1.6 fusion.116
  151.4 3.0 %reduce.15 = bf16[768,256]{1,0:T(8,128)(2,1)S(1)} reduce(bf16[768,1,256]{2,1,0:T(2,128)(2,1)S(1)} %bitcast.170, bf16[]{:T(256)} %broadcast.437), dimensions={1}, to_apply=%bitcast.127.reduce_sub_computation | reduce | bytes 786434
  155.3 3.5 %all-to-all-start = ((bf16[4,2,24576]{2,1,0:T(2,128)(2,1)}), bf16[4,2,24576]{2,1,0:T(2,128)(2,1)S(1)}, u32[]{:S(2)}, u32[]{:S(2)}) async-start(bf16[4,2,24576]{2,1,0:T(2,128)(2,1)} %reshape.681), calls=%async_computation | async-start | bytes 786432 | tf_op jit(solution)/shard_map/all_to_all | solution.py:171
  158.7 9.1 %all_gather.21 = f32[2,2048]{1,0:T(2,128)S(1)} all-gather(f32[2,512]{1,0:T(2,128)S(1)} %get-tuple-element.82), channel_id=1, replica_groups=mesh['sp'=4,'tp'=4,'dp'=2] {'tp'}, dimensions={1}, use_global_device_ids=true | all-gather | bytes 20480 | tf_op jit(solution)/shard_map/all_gather | solution.py:86
  168.7 4.1 %fusion.30 = bf16[1,192,2048]{2,1,0:T(8,128)(2,1)} fusion(bf16[192,1024]{1,0:T(8,128)(2,1)S(1)} %bitcast.181, bf16[1024,2048]{1,0:T(8,128)(2,1)} %param.31, bf16[1,192,2048]{2,1,0:T(8,128)(2,1)S(1)} %copy-done.1, f32[2048]{0:T(1024)S(1)} %bitcast.184), kind=kOutput, calls=%fused_computation.32 | convolution fusion | flops 806879232 | bytes 6168576 | tf_op jit(solution)/shard_map/srq,qd->srd/dot_general | solution.py:169
  (109 shorter events, 19.3 us)
Async XLA Ops:
  6.5 1.0 copy-start
  6.5 45.7 %copy-start.5 = (bf16[2048,64]{0,1:T(8,128)(2,1)S(1)}, bf16[2048,64]{0,1:T(8,128)(2,1)}, u32[]{:S(2)}) copy-start(bf16[2048,64]{0,1:T(8,128)(2,1)} %param.26) | copy-start | bytes 786436
  6.5 46.0 %copy-start.4 = (bf16[2048,64]{0,1:T(8,128)(2,1)S(1)}, bf16[2048,64]{0,1:T(8,128)(2,1)}, u32[]{:S(2)}) copy-start(bf16[2048,64]{0,1:T(8,128)(2,1)} %param.27) | copy-start | bytes 786436
  6.5 46.3 %copy-start.10 = (bf16[64]{0:T(256)(128)(2,1)S(1)}, bf16[64]{0:T(256)(128)(2,1)}, u32[]{:S(2)}) copy-start(bf16[64]{0:T(256)(128)(2,1)} %param.29) | copy-start | bytes 388
  6.5 46.3 %copy-start.11 = (bf16[64]{0:T(256)(128)(2,1)S(1)}, bf16[64]{0:T(256)(128)(2,1)}, u32[]{:S(2)}) copy-start(bf16[64]{0:T(256)(128)(2,1)} %param.28) | copy-start | bytes 388
  6.5 46.8 %copy-start.2 = (bf16[1,128,2048]{2,1,0:T(8,128)(2,1)S(1)}, bf16[1,128,2048]{2,1,0:T(8,128)(2,1)}, u32[]{:S(2)}) copy-start(bf16[1,128,2048]{2,1,0:T(8,128)(2,1)} %param.20) | copy-start | bytes 1572868
  6.6 86.9 %all-gather.3.cloned.1.call-start = ((), (), s32[]{:S(2)}) async-start(), calls=%async_computation.1 | async-start | bytes 3932160 | tf_op jit(solution)/shard_map/all_gather | solution.py:96
  81.2 17.6 %copy-start.9 = (f32[64]{0:T(128)S(1)}, f32[64]{0:T(128)}, u32[]{:S(2)}) copy-start(f32[64]{0:T(128)} %convert_element_type.121) | copy-start | bytes 772
  98.7 3.9 %copy-start.8 = (f32[4]{0:T(128)S(1)}, f32[4]{0:T(128)}, u32[]{:S(2)}) copy-start(f32[4]{0:T(128)} %param.30) | copy-start | bytes 52
  99.3 9.1 %collective-permute-start = (bf16[1,1,768,64]{2,3,1,0:T(8,128)(2,1)}, bf16[1,1,768,64]{2,3,1,0:T(8,128)(2,1)S(1)}, u32[]{:S(2)}, u32[]{:S(2)}) collective-permute-start(bf16[1,1,768,64]{2,3,1,0:T(8,128)(2,1)} %fusion.67), channel_id=1, source_target_pairs={{0,8},{8,16},{16,24},{24,0},{1,9},{9,17},{17,25},{25,1},{2,10},{10... | collective-permute-start | bytes 294920 | tf_op jit(solution)/shard_map/ppermute | solution.py:151
  104.4 1.4 copy-start.7
  105.8 1.5 copy-start.3
  105.8 1.5 copy-start.6
  108.5 6.5 %collective-permute-start.1 = (bf16[1,1,768,64]{2,3,1,0:T(8,128)(2,1)S(1)}, bf16[1,1,768,64]{2,3,1,0:T(8,128)(2,1)S(1)}, u32[]{:S(2)}, u32[]{:S(2)}) collective-permute-start(bf16[1,1,768,64]{2,3,1,0:T(8,128)(2,1)S(1)} %collective-permute-done), channel_id=1, source_target_pairs={{0,8},{8,16},{16,24},{24,0},{1,9},{9,17},{17,25},{25,1},{2,10},{10... | collective-permute-start | bytes 294920 | tf_op jit(solution)/shard_map/ppermute | solution.py:151
  114.9 15.1 %collective-permute-start.2 = (bf16[1,1,768,64]{2,3,1,0:T(8,128)(2,1)S(1)}, bf16[1,1,768,64]{2,3,1,0:T(8,128)(2,1)S(1)}, u32[]{:S(2)}, u32[]{:S(2)}) collective-permute-start(bf16[1,1,768,64]{2,3,1,0:T(8,128)(2,1)S(1)} %collective-permute-done.1), channel_id=1, source_target_pairs={{0,8},{8,16},{16,24},{24,0},{1,9},{9,17},{17,25},{25,1},{2,10},{10... | collective-permute-start | bytes 294920 | tf_op jit(solution)/shard_map/ppermute | solution.py:151
  150.3 18.4 %copy-start.1 = (bf16[1,192,2048]{2,1,0:T(8,128)(2,1)S(1)}, bf16[1,192,2048]{2,1,0:T(8,128)(2,1)}, u32[]{:S(2)}) copy-start(bf16[1,192,2048]{2,1,0:T(8,128)(2,1)} %param.17) | copy-start | bytes 2359300
  155.3 12.5 %all-to-all-start = ((bf16[4,2,24576]{2,1,0:T(2,128)(2,1)}), bf16[4,2,24576]{2,1,0:T(2,128)(2,1)S(1)}, u32[]{:S(2)}, u32[]{:S(2)}) async-start(bf16[4,2,24576]{2,1,0:T(2,128)(2,1)} %reshape.681), calls=%async_computation | async-start | bytes 786432 | tf_op jit(solution)/shard_map/all_to_all | solution.py:171
Sparse Core Ops, SparseCore 0:
  52.3 41.0 all-gather.2
